TPU v7x, 32 devices: a whole 2x2x4 slice. The times are simulated.
32 devices in a mesh: sp: 8 (over z, y), tp: 4 (over x, core).
Axes of the slice: x: 2, y: 2, z: 4, core: 2. Of those that a mesh axis runs over, the one named last changes fastest.
Arguments:
- queries: bfloat16 [4096, 1024], P('sp', 'tp'), may hold values from -200 to 200
- keys: bfloat16 [4096, 1024], P('sp', 'tp'), may hold values from -6 to 6
- values: bfloat16 [4096, 1024], P('sp', 'tp'), may hold values from -24 to 24
- cum_gate: float32 [4096, 8], P('sp', 'tp'), may hold values from -414 to 0, as said below
- residual: bfloat16 [4096, 2048], P(('sp', 'tp')), may hold values from -1.5 to 1.5
- w_out: bfloat16 [1024, 2048], replicated, may hold values from -0.1875 to 0.1875
- gain: float32 [2048], replicated, may hold values from 0.1 to 1.9
- w_up: bfloat16 [2048, 8192], P('sp', 'tp'), may hold values from -0.125 to 0.125
- w_down: bfloat16 [8192, 2048], P('tp', 'sp'), may hold values from -0.0625 to 0.0625
Outputs:
- output: bfloat16 [4096, 2048], P(('sp', 'tp'))
Inputs may be any that keep to these rules, and one draw needn't show every extreme that they name: Within each head, cum_gate never rises from one position to the next.
All inputs are finite; a program needn't handle non-finite values.
Results may differ from a plain program's by a relative error of at most 0.022.
Values may be sent and summed in bfloat16 or wider, within the bound.
A program may use at most 128 MiB of HBM per device.

v0:
```python
import math
import jax
import jax.numpy as jnp
from jax import lax
from jax.sharding import PartitionSpec as P


def per_device(queries, keys, values, cum_gate, residual, w_out, gain, w_up, w_down):
    tok_rows, width = queries.shape
    heads_here = cum_gate.shape[1]
    head_size = width // heads_here
    score_scale = head_size ** (-0.5)
    row_offset = lax.axis_index("sp") * tok_rows
    query_heads = queries.reshape(tok_rows, heads_here, head_size)
    query_pos = row_offset + jnp.arange(tok_rows, dtype=jnp.int32)
    all_gates = lax.all_gather(cum_gate, "sp", axis=0, tiled=True)
    initial = (
        jnp.full((tok_rows, heads_here), -1e30, jnp.float32),
        jnp.zeros((tok_rows, heads_here), jnp.float32),
        jnp.zeros((tok_rows, heads_here, head_size), jnp.float32),
    )
    carried = initial
    key_rows = lax.all_gather(keys, "sp", axis=0, tiled=True)
    value_rows = lax.all_gather(values, "sp", axis=0, tiled=True)
    row_count = key_rows.shape[0]
    span_rows = math.gcd(row_count, 2048)
    block_count = row_count // span_rows
    key_blocks = key_rows.reshape(block_count, span_rows, heads_here, head_size)
    value_blocks = value_rows.reshape(block_count, span_rows, heads_here, head_size)
    first_pos = jnp.arange(block_count, dtype=jnp.int32) * span_rows

    def absorb_block(running, packed):
        running_max, running_sum, accumulated = running
        key_blk, value_blk, block_start = packed
        gate_blk = lax.dynamic_slice_in_dim(all_gates, block_start, span_rows, 0)
        scores = jnp.einsum(
            "qhd,khd->qhk", query_heads, key_blk, preferred_element_type=jnp.float32
        )
        scores = scores * score_scale + cum_gate[:, :, None] - gate_blk.T[None, :, :]
        key_pos = block_start + jnp.arange(span_rows, dtype=jnp.int32)
        scores = jnp.where(key_pos[None, None, :] <= query_pos[:, None, None], scores, -1e30)
        new_max = jnp.maximum(running_max, jnp.max(scores, axis=-1))
        rescale = jnp.exp(running_max - new_max)
        weights = jnp.exp(scores - new_max[:, :, None])
        running_sum = running_sum * rescale + jnp.sum(weights, axis=-1)
        product = jnp.einsum(
            "qhk,khd->qhd",
            weights.astype(jnp.bfloat16),
            value_blk,
            preferred_element_type=jnp.float32,
        )
        accumulated = accumulated * rescale[:, :, None] + product
        return ((new_max, running_sum, accumulated), None)

    carried, _ = lax.scan(absorb_block, carried, (key_blocks, value_blocks, first_pos))
    running_max, running_sum, accumulated = carried
    attended = (accumulated / running_sum[:, :, None]).reshape(tok_rows, width).astype(jnp.bfloat16)
    mine = lax.all_to_all(attended, "tp", split_axis=0, concat_axis=1, tiled=True)
    projected = jnp.dot(mine, w_out, preferred_element_type=jnp.float32)
    residual_sum = residual.astype(jnp.float32) + projected
    mean_square = jnp.mean(residual_sum * residual_sum, axis=-1, keepdims=True)
    normed = (residual_sum * lax.rsqrt(mean_square + 1e-06) * gain).astype(jnp.bfloat16)
    normed_all = lax.all_gather(normed, "tp", axis=0, tiled=True)
    up_proj = jnp.dot(
        normed_all,
        lax.all_gather(w_up, "sp", axis=0, tiled=True),
        preferred_element_type=jnp.float32,
    )
    hidden = jnp.square(jax.nn.relu(up_proj)).astype(jnp.bfloat16)
    down_whole = lax.all_gather(w_down, "sp", axis=1, tiled=True)
    rounded = jnp.dot(hidden, down_whole, preferred_element_type=jnp.float32).astype(jnp.bfloat16)
    branch_out = lax.psum_scatter(
        lax.optimization_barrier(rounded).astype(jnp.float32).astype(jnp.bfloat16),
        "tp",
        scatter_dimension=0,
        tiled=True,
    ).astype(jnp.float32)
    return (residual_sum + branch_out).astype(jnp.bfloat16)


def solution(mesh):
    return jax.shard_map(
        per_device,
        mesh=mesh,
        in_specs=(
            P("sp", "tp"),
            P("sp", "tp"),
            P("sp", "tp"),
            P("sp", "tp"),
            P(("sp", "tp"), None),
            P(),
            P(),
            P("sp", "tp"),
            P("tp", "sp"),
        ),
        out_specs=P(("sp", "tp"), None),
        check_vma=False,
    )
```

profile of v0, /device:TPU:0, one launch (start us, length us, event | category | flops | bytes accessed | tf_op | source)
XLA Modules:
  0.0 501.9 jit_solution(15590965651173478988)
XLA Ops:
  6.5 0.0 copy-start
  6.5 0.0 all-gather.6.cloned.1.call-start
  6.5 0.7 all-gather.6.cloned.1.call-update
  7.3 0.0 all-gather.8.cloned.1.call-start
  7.3 0.7 all-gather.8.cloned.1.call-update
  8.0 0.0 all-gather.10.cloned.1.call-start
  8.1 1.1 copy.17
  9.2 0.2 copy.19
  9.4 32.7 %all_gather.19 = f32[4096,2]{0,1:T(2,128)S(1)} all-gather(f32[512,2]{0,1:T(2,128)} %param.14), channel_id=1, replica_groups=mesh['sp'=8,'tp'=4] {'sp'}, dimensions={0}, use_global_device_ids=true | all-gather | bytes 36864 | tf_op jit(solution)/shard_map/all_gather | solution.py:16
  42.0 19.4 %all-gather.6.cloned.1.call-done = bf16[4096,256]{1,0:T(8,128)(2,1)} async-done(((bf16[512,256]{1,0:T(8,128)(2,1)}), bf16[4096,256]{1,0:T(8,128)(2,1)}) %all-gather.6.cloned.1.call-update) | async-done | bytes 2097168 | tf_op jit(solution)/shard_map/all_gather | solution.py:23
  61.4 4.0 reshape.62
  65.4 45.8 %all-gather.8.cloned.1.call-done = bf16[4096,256]{1,0:T(8,128)(2,1)} async-done(((bf16[512,256]{1,0:T(8,128)(2,1)}), bf16[4096,256]{1,0:T(8,128)(2,1)}) %all-gather.8.cloned.1.call-update) | async-done | bytes 2097168 | tf_op jit(solution)/shard_map/all_gather | solution.py:24
  111.2 4.0 reshape.64
  115.2 0.0 copy-done
  115.2 45.9 %while.15 = (s32[]{:T(128)}, f32[512,2]{0,1:T(2,128)S(1)}, f32[512,2]{0,1:T(2,128)S(1)}, f32[512,2,128]{0,2,1:T(8,128)}, s32[2]{0:T(128)S(1)}, /*index=5*/bf16[2...) while((s32[]{:T(128)}, f32[512,2]{0,1:T(2,128)S(1)}, ...), condition=%wide.region_3.4_spmd.clone, body=%wide.region_0.3_spmd.clone.sunk | while | flops 1110842880 | bytes 39239884 | solution.py:55
  115.2 0.6 dynamic_slice.26
  117.4 0.1 dynamic-slice_bitcast_fusion.2
  117.5 0.6 iota_add_fusion.5
  118.1 0.8 broadcast_compare_fusion.2
  118.9 2.7 constant_dynamic-slice_fusion.3
  121.6 4.6 fusion.40
  126.2 4.8 fusion.42
  131.0 0.8 copy.34
  131.8 6.2 %fusion.44 = f32[512,2,128]{0,2,1:T(8,128)} fusion(f32[2,2048,512]{2,1,0:T(8,128)} %get-tuple-element.231, f32[512,2]{0,1:T(2,128)S(1)} %fusion.41, f32[2,2048]{1,0:T(2,128)S(1)} %dynamic-slice_bitcast_fusion.2, f32[512,2]{0,1:T(2,128)S(1)} %get-tuple-element.270, pred[512,2048]{0,1:T(8,128)(4,1)S(1)} %broadcast_compare_fusion.2, ...), kind=kOutput, calls=%fused_computation.12.clone.1 | convolution fusion | flops 549847040 | bytes 11563009 | tf_op jit(solution)/shard_map/while/body/eval_jaxpr/qhk,khd->qhd/dot_general | solution.py:46
  138.1 0.6 dynamic_slice.26
  140.3 0.1 dynamic-slice_bitcast_fusion.2
  140.4 0.6 iota_add_fusion.5
  141.0 0.8 broadcast_compare_fusion.2
  141.8 2.7 constant_dynamic-slice_fusion.3
  144.5 4.6 fusion.40
  149.1 4.8 fusion.42
  153.9 0.8 copy.34
  154.7 6.4 %fusion.44 = f32[512,2,128]{0,2,1:T(8,128)} fusion(f32[2,2048,512]{2,1,0:T(8,128)} %get-tuple-element.231, f32[512,2]{0,1:T(2,128)S(1)} %fusion.41, f32[2,2048]{1,0:T(2,128)S(1)} %dynamic-slice_bitcast_fusion.2, f32[512,2]{0,1:T(2,128)S(1)} %get-tuple-element.270, pred[512,2048]{0,1:T(8,128)(4,1)S(1)} %broadcast_compare_fusion.2, ...), kind=kOutput, calls=%fused_computation.12.clone.1 | convolution fusion | flops 549847040 | bytes 11563009 | tf_op jit(solution)/shard_map/while/body/eval_jaxpr/qhk,khd->qhd/dot_general | solution.py:46
  161.1 0.0 copy-start.1
  161.1 1.1 divide_convert_fusion
  162.2 0.1 reshape.65
  162.2 0.2 copy.24
  162.4 8.5 %all_to_all.16 = bf16[4,128,256]{2,1,0:T(8,128)(2,1)S(1)} all-to-all(bf16[4,128,256]{2,1,0:T(8,128)(2,1)S(1)} %copy.24), channel_id=1, replica_groups=mesh['sp'=8,'tp'=4] {'tp'}, dimensions={0} | all-to-all | bytes 524288 | tf_op jit(solution)/shard_map/all_to_all | solution.py:58
  171.0 0.2 copy.22
  171.1 3.1 multiply_reduce_fusion
  174.3 0.0 copy-done.1
  174.3 0.9 multiply_convert_fusion.1
  175.2 0.0 all-gather.10.cloned.1.call-update
  175.3 0.0 all-gather.12.cloned.1.call-start
  175.3 0.5 all-gather.12.cloned.1.call-update
  175.8 0.0 all-gather.14.cloned.1.call-start
  175.9 0.5 all-gather.14.cloned.1.call-update
  176.4 0.2 reduce-scatter.2.cloned.1.call-start
  176.7 19.0 %all-gather.10.cloned.1.call-done = bf16[512,2048]{1,0:T(8,128)(2,1)} async-done(((bf16[128,2048]{1,0:T(8,128)(2,1)}), bf16[512,2048]{1,0:T(8,128)(2,1)}) %all-gather.10.cloned.1.call-update) | async-done | bytes 2097168 | tf_op jit(solution)/shard_map/all_gather | solution.py:63
  195.6 126.5 %all-gather.12.cloned.1.call-done = bf16[2048,2048]{1,0:T(8,128)(2,1)} async-done(((bf16[256,2048]{1,0:T(8,128)(2,1)}), bf16[2048,2048]{1,0:T(8,128)(2,1)}) %all-gather.12.cloned.1.call-update) | async-done | bytes 8388624 | tf_op jit(solution)/shard_map/all_gather | solution.py:66
  322.1 125.0 %all-gather.14.cloned.1.call-done = bf16[2048,2048]{1,0:T(8,128)(2,1)} async-done(((bf16[2048,256]{1,0:T(8,128)(2,1)}), bf16[2048,2048]{1,0:T(8,128)(2,1)}) %all-gather.14.cloned.1.call-update) | async-done | bytes 8388624 | tf_op jit(solution)/shard_map/all_gather | solution.py:70
  447.1 16.5 %convolution_convert_fusion = bf16[512,2048]{1,0:T(8,128)(2,1)} fusion(bf16[2048,2048]{1,0:T(8,128)(2,1)} %all-gather.14.cloned.1.call-done, bf16[512,2048]{1,0:T(8,128)(2,1)} %all-gather.10.cloned.1.call-done, bf16[2048,2048]{1,0:T(8,128)(2,1)} %all-gather.12.cloned.1.call-done), kind=kOutput, calls=%fused_computation.30 | convolution fusion | flops 8594128896 | bytes 20971520 | tf_op jit(solution)/shard_map/dot_general | solution.py:71
  463.7 0.0 reduce-scatter.2.cloned.1.call-update
  463.7 29.5 %reduce-scatter.2.cloned.1.call-done = bf16[128,2048]{1,0:T(8,128)(2,1)} async-done(((bf16[512,2048]{1,0:T(8,128)(2,1)}), bf16[128,2048]{1,0:T(8,128)(2,1)}) %reduce-scatter.2.cloned.1.call-update) | async-done | bytes 524304 | tf_op jit(solution)/shard_map/reduce_scatter | solution.py:72
  493.2 1.9 add_convert_fusion
  (13 shorter events, 0.1 us)
Async XLA Ops:
  6.5 108.6 %copy-start = (f32[512,2]{0,1:T(2,128)S(1)}, f32[512,2]{0,1:T(2,128)}, u32[]{:S(2)}) copy-start(f32[512,2]{0,1:T(2,128)} %param.14) | copy-start | bytes 12292
  6.5 54.9 %all-gather.6.cloned.1.call-start = ((), (), s32[]{:S(2)}) async-start(), calls=%async_computation.2 | async-start | bytes 2359296 | tf_op jit(solution)/shard_map/all_gather | solution.py:23
  7.3 103.9 %all-gather.8.cloned.1.call-start = ((), (), s32[]{:S(2)}) async-start(), calls=%async_computation.3 | async-start | bytes 2359296 | tf_op jit(solution)/shard_map/all_gather | solution.py:24
  8.0 187.6 %all-gather.10.cloned.1.call-start = ((), (), s32[]{:S(2)}) async-start(), calls=%async_computation.4 | async-start | bytes 2621440 | tf_op jit(solution)/shard_map/all_gather | solution.py:63
  161.1 13.2 %copy-start.1 = (f32[2048]{0:T(1024)S(1)}, f32[2048]{0:T(1024)}, u32[]{:S(2)}) copy-start(f32[2048]{0:T(1024)} %param.17) | copy-start | bytes 24580
  175.3 146.8 %all-gather.12.cloned.1.call-start = ((), (), s32[]{:S(2)}) async-start(), calls=%async_computation.5 | async-start | bytes 9437184 | tf_op jit(solution)/shard_map/all_gather | solution.py:66
  175.8 271.3 %all-gather.14.cloned.1.call-start = ((), (), s32[]{:S(2)}) async-start(), calls=%async_computation.6 | async-start | bytes 9437184 | tf_op jit(solution)/shard_map/all_gather | solution.py:70
  176.4 316.7 %reduce-scatter.2.cloned.1.call-start = ((), (), s32[]{:S(2)}) async-start(), calls=%async_computation.7 | async-start | bytes 2621440 | tf_op jit(solution)/shard_map/reduce_scatter | solution.py:72
Sparse Core Ops, SparseCore 0:
  9.5 51.9 all-gather.5
  63.5 47.6 all-gather.7
  175.4 20.1 all-gather.9
  197.6 124.4 all-gather.11
  324.0 123.1 all-gather.13
  463.8 29.3 reduce-scatter.1
where the time goes:
time: 502 us
  waiting for transfers between devices  368 us (73%)
  matrix products  41.4 us (8%)
  blocking collectives  41.2 us (8%)
  local copies, waits for them, and re-layouts  18 us (4%)
  other arithmetic  16.3 us (3%)
  between operations  13.6 us (3%)
    all_gather x1, waiting for transfers between devices, per_device(): lax.all_gather(w_up, 'sp', axis=0, tiled=True)  126 us
    all_gather x1, waiting for transfers between devices, per_device(): down_whole = lax.all_gather(w_down, 'sp', axis=1, tiled=True)  125 us
    all_gather x1, waiting for transfers between devices, per_device(): value_rows = lax.all_gather(values, 'sp', axis=0, tiled=True)  45.8 us
    all_gather x1, blocking collectives, per_device(): all_gates = lax.all_gather(cum_gate, 'sp', axis=0, tiled=True)  32.7 us
    reduce_scatter x1, waiting for transfers between devices, per_device(): lax.psum_scatter(lax.optimization_barrier(rounded).astype(jnp.float32).as...  29.5 us
    all_gather x1, waiting for transfers between devices, per_device(): key_rows = lax.all_gather(keys, 'sp', axis=0, tiled=True)  19.4 us
    all_gather x1, waiting for transfers between devices, per_device(): normed_all = lax.all_gather(normed, 'tp', axis=0, tiled=True)  19 us
    dot_general x1, matrix products, per_device(): jnp.dot(hidden, down_whole, preferred_element_type=jnp.float32)  16.5 us
  transfers between devices with their start and end apart: 6, of which 6 were waited for; matrix products, arithmetic and copies ran while one was open for 1% of the time, Pallas kernels for 0%

commit v1 on v0

--- a/solution.py
+++ b/solution.py
@@ -67,7 +67,12 @@
         preferred_element_type=jnp.float32,
     )
     hidden = jnp.square(jax.nn.relu(up_proj)).astype(jnp.bfloat16)
-    down_whole = lax.all_gather(w_down, "sp", axis=1, tiled=True)
+    ring = [w_down]
+    for hop in range(7):
+        ring.append(lax.ppermute(ring[-1], "sp", [(dev, (dev + 1) % 8) for dev in range(8)]))
+    down_whole = jnp.roll(
+        jnp.concatenate(ring[::-1], axis=1), (lax.axis_index("sp") + 1) * ring[0].shape[1], axis=1
+    )
     rounded = jnp.dot(hidden, down_whole, preferred_element_type=jnp.float32).astype(jnp.bfloat16)
     branch_out = lax.psum_scatter(
         lax.optimization_barrier(rounded).astype(jnp.float32).astype(jnp.bfloat16),

time: 502 us -> 525 us (1.046)
  local copies, waits for them, and re-layouts: 18 us -> 47.1 us
  waiting for transfers between devices: 368 us -> 361 us
    ppermute x0 -> x7, waiting for transfers between devices: none -> 265 us  [per_device(): lax.ppermute(ring[-1], 'sp', [(dev, (dev + 1) % 8) for dev in range(8)])]
    all_gather x1, waiting for transfers between devices: 126 us -> 0.01 us  [per_device(): lax.all_gather(w_up, 'sp', axis=0, tiled=True)]
    all_gather x1 -> x0, waiting for transfers between devices: 125 us -> none  [per_device(): down_whole = lax.all_gather(w_down, 'sp', axis=1, tiled=True)]
    unnamed x6 -> x39, local copies, waits for them, and re-layouts: 1.27 us -> 29.2 us
    all_gather x1, waiting for transfers between devices: 19 us -> 0.01 us  [per_device(): normed_all = lax.all_gather(normed, 'tp', axis=0, tiled=True)]
  transfers between devices with their start and end apart: 6 -> 12, of which waited for: 6 -> 10; matrix products, arithmetic and copies ran while one was open for 1% -> 6% of each run, Pallas kernels for 0% -> 0%
where the time goes in v1:
time: 525 us
  waiting for transfers between devices  361 us (69%)
  local copies, waits for them, and re-layouts  47.1 us (9%)
  matrix products  41.6 us (8%)
  blocking collectives  41.2 us (8%)
  other arithmetic  16.4 us (3%)
  between operations  13.3 us (3%)
    ppermute x7, waiting for transfers between devices, per_device(): lax.ppermute(ring[-1], 'sp', [(dev, (dev + 1) % 8) for dev in range(8)])  265 us
    all_gather x1, waiting for transfers between devices, per_device(): value_rows = lax.all_gather(values, 'sp', axis=0, tiled=True)  45.7 us
    all_gather x1, blocking collectives, per_device(): all_gates = lax.all_gather(cum_gate, 'sp', axis=0, tiled=True)  32.7 us
    unnamed x39, local copies, waits for them, and re-layouts  29.2 us
    reduce_scatter x1, waiting for transfers between devices, per_device(): lax.psum_scatter(lax.optimization_barrier(rounded).astype(jnp.float32).as...  29 us
    all_gather x1, waiting for transfers between devices, per_device(): key_rows = lax.all_gather(keys, 'sp', axis=0, tiled=True)  19.4 us
    dot_general x1, matrix products, per_device(): jnp.dot(hidden, down_whole, preferred_element_type=jnp.float32)  16.5 us
    dot_general x2, matrix products, absorb_block(): jnp.einsum('qhk,khd->qhd', weights.astype(jnp.bfloat16), value_blk, prefe...  12.6 us
  transfers between devices with their start and end apart: 12, of which 10 were waited for; matrix products, arithmetic and copies ran while one was open for 6% of the time, Pallas kernels for 0%

profile of v1, /device:TPU:0, one launch (start us, length us, event | category | flops | bytes accessed | tf_op | source)
XLA Modules:
  0.0 524.7 jit_solution(5509641298809806234)
XLA Ops:
  6.5 0.7 all-gather.5.cloned.1.call-update
  7.3 0.7 all-gather.7.cloned.1.call-update
  8.1 1.1 copy.17
  9.2 0.2 copy.19
  9.4 32.7 %all_gather.16 = f32[4096,2]{0,1:T(2,128)S(1)} all-gather(f32[512,2]{0,1:T(2,128)} %param.14), channel_id=1, replica_groups=mesh['sp'=8,'tp'=4] {'sp'}, dimensions={0}, use_global_device_ids=true | all-gather | bytes 36864 | tf_op jit(solution)/shard_map/all_gather | solution.py:16
  42.0 19.4 %all-gather.5.cloned.1.call-done = bf16[4096,256]{1,0:T(8,128)(2,1)} async-done(((bf16[512,256]{1,0:T(8,128)(2,1)}), bf16[4096,256]{1,0:T(8,128)(2,1)}) %all-gather.5.cloned.1.call-update) | async-done | bytes 2097168 | tf_op jit(solution)/shard_map/all_gather | solution.py:23
  61.4 4.1 reshape.62
  65.5 45.7 %all-gather.7.cloned.1.call-done = bf16[4096,256]{1,0:T(8,128)(2,1)} async-done(((bf16[512,256]{1,0:T(8,128)(2,1)}), bf16[4096,256]{1,0:T(8,128)(2,1)}) %all-gather.7.cloned.1.call-update) | async-done | bytes 2097168 | tf_op jit(solution)/shard_map/all_gather | solution.py:24
  111.2 4.0 reshape.64
  115.2 46.1 %while.15 = (s32[]{:T(128)}, f32[512,2]{0,1:T(2,128)S(1)}, f32[512,2]{0,1:T(2,128)S(1)}, f32[512,2,128]{0,2,1:T(8,128)}, s32[2]{0:T(128)S(1)}, /*index=5*/bf16[2...) while((s32[]{:T(128)}, f32[512,2]{0,1:T(2,128)S(1)}, ...), condition=%wide.region_3.4_spmd.clone, body=%wide.region_0.3_spmd.clone.sunk | while | flops 1110842880 | bytes 39239884 | solution.py:55
  115.2 0.6 dynamic_slice.35
  117.6 0.6 iota_add_fusion.5
  118.2 0.8 broadcast_compare_fusion.2
  119.0 2.7 constant_dynamic-slice_fusion.3
  121.6 4.6 fusion.45
  126.3 4.8 fusion.47
  131.1 0.8 copy.34
  131.9 6.2 %fusion.49 = f32[512,2,128]{0,2,1:T(8,128)} fusion(f32[2,2048,512]{2,1,0:T(8,128)} %get-tuple-element.231, f32[512,2]{0,1:T(2,128)S(1)} %fusion.46, f32[2,2048]{1,0:T(2,128)S(1)} %dynamic-slice_bitcast_fusion.2, f32[512,2]{0,1:T(2,128)S(1)} %get-tuple-element.270, pred[512,2048]{0,1:T(8,128)(4,1)S(1)} %broadcast_compare_fusion.2, ...), kind=kOutput, calls=%fused_computation.12.clone.1 | convolution fusion | flops 549847040 | bytes 11563009 | tf_op jit(solution)/shard_map/while/body/eval_jaxpr/qhk,khd->qhd/dot_general | solution.py:46
  138.2 0.6 dynamic_slice.35
  140.6 0.6 iota_add_fusion.5
  141.2 0.8 broadcast_compare_fusion.2
  141.9 2.7 constant_dynamic-slice_fusion.3
  144.6 4.7 fusion.45
  149.3 4.8 fusion.47
  154.1 0.8 copy.34
  154.9 6.4 %fusion.49 = f32[512,2,128]{0,2,1:T(8,128)} fusion(f32[2,2048,512]{2,1,0:T(8,128)} %get-tuple-element.231, f32[512,2]{0,1:T(2,128)S(1)} %fusion.46, f32[2,2048]{1,0:T(2,128)S(1)} %dynamic-slice_bitcast_fusion.2, f32[512,2]{0,1:T(2,128)S(1)} %get-tuple-element.270, pred[512,2048]{0,1:T(8,128)(4,1)S(1)} %broadcast_compare_fusion.2, ...), kind=kOutput, calls=%fused_computation.12.clone.1 | convolution fusion | flops 549847040 | bytes 11563009 | tf_op jit(solution)/shard_map/while/body/eval_jaxpr/qhk,khd->qhd/dot_general | solution.py:46
  161.3 1.2 divide_convert_fusion
  162.5 0.2 copy.24
  162.7 8.5 %all_to_all.16 = bf16[4,128,256]{2,1,0:T(8,128)(2,1)S(1)} all-to-all(bf16[4,128,256]{2,1,0:T(8,128)(2,1)S(1)} %copy.24), channel_id=1, replica_groups=mesh['sp'=8,'tp'=4] {'tp'}, dimensions={0} | all-to-all | bytes 524288 | tf_op jit(solution)/shard_map/all_to_all | solution.py:58
  171.2 0.2 copy.22
  171.4 3.1 multiply_reduce_fusion
  174.6 0.9 multiply_convert_fusion.1
  175.6 0.5 all-gather.11.cloned.1.call-update
  176.2 0.6 collective-permute-start
  176.8 26.7 %collective-permute-done = bf16[2048,256]{1,0:T(8,128)(2,1)S(1)} collective-permute-done((bf16[2048,256]{1,0:T(8,128)(2,1)S(1)}, bf16[2048,256]{1,0:T(8,128)(2,1)S(1)}, u32[]{:S(2)}, u32[]{:S(2)}) %collective-permute-start) | collective-permute-done | bytes 1048608 | tf_op jit(solution)/shard_map/ppermute | solution.py:72
  203.5 46.6 %collective-permute-done.1 = bf16[2048,256]{1,0:T(8,128)(2,1)S(1)} collective-permute-done((bf16[2048,256]{1,0:T(8,128)(2,1)S(1)}, bf16[2048,256]{1,0:T(8,128)(2,1)S(1)}, u32[]{:S(2)}, u32[]{:S(2)}) %collective-permute-start.1) | collective-permute-done | bytes 1048608 | tf_op jit(solution)/shard_map/ppermute | solution.py:72
  250.0 1.0 copy-done.1
  251.1 41.5 %collective-permute-done.2 = bf16[2048,256]{1,0:T(8,128)(2,1)S(1)} collective-permute-done((bf16[2048,256]{1,0:T(8,128)(2,1)S(1)}, bf16[2048,256]{1,0:T(8,128)(2,1)S(1)}, u32[]{:S(2)}, u32[]{:S(2)}) %collective-permute-start.2) | collective-permute-done | bytes 1048608 | tf_op jit(solution)/shard_map/ppermute | solution.py:72
  292.6 1.0 copy-done.3
  293.6 49.1 %collective-permute-done.3 = bf16[2048,256]{1,0:T(8,128)(2,1)S(1)} collective-permute-done((bf16[2048,256]{1,0:T(8,128)(2,1)S(1)}, bf16[2048,256]{1,0:T(8,128)(2,1)S(1)}, u32[]{:S(2)}, u32[]{:S(2)}) %collective-permute-start.3) | collective-permute-done | bytes 1048608 | tf_op jit(solution)/shard_map/ppermute | solution.py:72
  342.7 1.0 copy-done.5
  343.7 49.1 %collective-permute-done.4 = bf16[2048,256]{1,0:T(8,128)(2,1)S(1)} collective-permute-done((bf16[2048,256]{1,0:T(8,128)(2,1)S(1)}, bf16[2048,256]{1,0:T(8,128)(2,1)S(1)}, u32[]{:S(2)}, u32[]{:S(2)}) %collective-permute-start.4) | collective-permute-done | bytes 1048608 | tf_op jit(solution)/shard_map/ppermute | solution.py:72
  392.7 1.0 copy-done.7
  393.7 27.3 %collective-permute-done.5 = bf16[2048,256]{1,0:T(8,128)(2,1)} collective-permute-done((bf16[2048,256]{1,0:T(8,128)(2,1)S(1)}, bf16[2048,256]{1,0:T(8,128)(2,1)}, u32[]{:S(2)}, u32[]{:S(2)}) %collective-permute-start.5) | collective-permute-done | bytes 1048608 | tf_op jit(solution)/shard_map/ppermute | solution.py:72
  421.0 24.7 %collective-permute-done.6 = bf16[2048,256]{1,0:T(8,128)(2,1)} collective-permute-done((bf16[2048,256]{1,0:T(8,128)(2,1)}, bf16[2048,256]{1,0:T(8,128)(2,1)}, u32[]{:S(2)}, u32[]{:S(2)}) %collective-permute-start.6) | collective-permute-done | bytes 1048608 | tf_op jit(solution)/shard_map/ppermute | solution.py:72
  445.7 2.3 constant_dynamic-update-slice_fusion.15
  448.1 2.3 constant_dynamic-update-slice_fusion.14
  450.4 2.4 constant_dynamic-update-slice_fusion.13
  452.8 2.4 constant_dynamic-update-slice_fusion.12
  455.2 1.1 constant_dynamic-update-slice_fusion.11
  456.3 1.1 constant_dynamic-update-slice_fusion.10
  457.4 1.1 constant_dynamic-update-slice_fusion.9
  458.5 1.1 constant_dynamic-update-slice_fusion.8
  459.6 2.3 constant_dynamic-update-slice_fusion.7
  461.9 2.3 constant_dynamic-update-slice_fusion.6
  464.2 1.1 constant_dynamic-update-slice_fusion.5
  465.3 1.1 constant_dynamic-update-slice_fusion.4
  466.4 1.1 constant_dynamic-update-slice_fusion.3
  467.5 1.1 constant_dynamic-update-slice_fusion.2
  468.6 1.1 constant_dynamic-update-slice_fusion.1
  469.7 1.1 constant_dynamic-update-slice_fusion
  470.8 16.5 %fusion.24 = bf16[512,2048]{1,0:T(8,128)(2,1)} fusion(bf16[2048,4096]{1,0:T(8,128)(2,1)} %constant_dynamic-update-slice_fusion, s32[]{:T(128)S(6)} %select_n.21, bf16[512,2048]{1,0:T(8,128)(2,1)} %all-gather.9.cloned.1.call-done, bf16[2048,2048]{1,0:T(8,128)(2,1)} %all-gather.11.cloned.1.call-done), kind=kOutput, calls=%fused_computation.32 | convolution fusion | flops 8594128896 | bytes 20971524 | tf_op jit(solution)/shard_map/dot_general | solution.py:76
  487.3 29.0 %reduce-scatter.2.cloned.1.call-done = bf16[128,2048]{1,0:T(8,128)(2,1)} async-done(((bf16[512,2048]{1,0:T(8,128)(2,1)}), bf16[128,2048]{1,0:T(8,128)(2,1)}) %reduce-scatter.2.cloned.1.call-update) | async-done | bytes 524304 | tf_op jit(solution)/shard_map/reduce_scatter | solution.py:77
  516.3 1.9 add_convert_fusion
  (49 shorter events, 0.6 us)
Async XLA Ops:
  6.5 108.7 %copy-start.9 = (f32[512,2]{0,1:T(2,128)S(1)}, f32[512,2]{0,1:T(2,128)}, u32[]{:S(2)}) copy-start(f32[512,2]{0,1:T(2,128)} %param.14) | copy-start | bytes 12292
  6.5 54.9 %all-gather.5.cloned.1.call-start = ((), (), s32[]{:S(2)}) async-start(), calls=%async_computation.2 | async-start | bytes 2359296 | tf_op jit(solution)/shard_map/all_gather | solution.py:23
  7.3 103.9 %all-gather.7.cloned.1.call-start = ((), (), s32[]{:S(2)}) async-start(), calls=%async_computation.3 | async-start | bytes 2359296 | tf_op jit(solution)/shard_map/all_gather | solution.py:24
  8.0 462.8 %all-gather.9.cloned.1.call-start = ((), (), s32[]{:S(2)}) async-start(), calls=%async_computation.4 | async-start | bytes 2621440 | tf_op jit(solution)/shard_map/all_gather | solution.py:63
  161.3 13.3 %copy-start.10 = (f32[2048]{0:T(1024)S(1)}, f32[2048]{0:T(1024)}, u32[]{:S(2)}) copy-start(f32[2048]{0:T(1024)} %param.17) | copy-start | bytes 24580
  161.3 14.9 %copy-start = (bf16[2048,256]{1,0:T(8,128)(2,1)S(1)}, bf16[2048,256]{1,0:T(8,128)(2,1)}, u32[]{:S(2)}) copy-start(bf16[2048,256]{1,0:T(8,128)(2,1)} %param.19) | copy-start | bytes 3145732
  175.5 295.2 %all-gather.11.cloned.1.call-start = ((), (), s32[]{:S(2)}) async-start(), calls=%async_computation.5 | async-start | bytes 9437184 | tf_op jit(solution)/shard_map/all_gather | solution.py:66
  176.1 340.1 %reduce-scatter.2.cloned.1.call-start = ((), (), s32[]{:S(2)}) async-start(), calls=%async_computation.6 | async-start | bytes 2621440 | tf_op jit(solution)/shard_map/reduce_scatter | solution.py:77
  176.2 27.3 %collective-permute-start = (bf16[2048,256]{1,0:T(8,128)(2,1)S(1)}, bf16[2048,256]{1,0:T(8,128)(2,1)S(1)}, u32[]{:S(2)}, u32[]{:S(2)}) collective-permute-start(bf16[2048,256]{1,0:T(8,128)(2,1)S(1)} %copy-done), channel_id=1, source_target_pairs={{0,4},{4,8},{8,12},{12,16},{16,20},{20,24},{24,28},{28,0},{1,5},{5... | collective-permute-start | bytes 3145736 | tf_op jit(solution)/shard_map/ppermute | solution.py:72
  203.5 46.6 %collective-permute-start.1 = (bf16[2048,256]{1,0:T(8,128)(2,1)S(1)}, bf16[2048,256]{1,0:T(8,128)(2,1)S(1)}, u32[]{:S(2)}, u32[]{:S(2)}) collective-permute-start(bf16[2048,256]{1,0:T(8,128)(2,1)S(1)} %collective-permute-done), channel_id=1, source_target_pairs={{0,4},{4,8},{8,12},{12,16},{16,20},{20,24},{24,28},{28,0},{1,5},{5... | collective-permute-start | bytes 3145736 | tf_op jit(solution)/shard_map/ppermute | solution.py:72
  250.0 1.0 copy-start.1
  251.1 41.5 %collective-permute-start.2 = (bf16[2048,256]{1,0:T(8,128)(2,1)S(1)}, bf16[2048,256]{1,0:T(8,128)(2,1)S(1)}, u32[]{:S(2)}, u32[]{:S(2)}) collective-permute-start(bf16[2048,256]{1,0:T(8,128)(2,1)S(1)} %collective-permute-done.1), channel_id=1, source_target_pairs={{0,4},{4,8},{8,12},{12,16},{16,20},{20,24},{24,28},{28,0},{1,5},{5... | collective-permute-start | bytes 3145736 | tf_op jit(solution)/shard_map/ppermute | solution.py:72
  292.6 1.0 copy-start.3
  293.6 49.1 %collective-permute-start.3 = (bf16[2048,256]{1,0:T(8,128)(2,1)S(1)}, bf16[2048,256]{1,0:T(8,128)(2,1)S(1)}, u32[]{:S(2)}, u32[]{:S(2)}) collective-permute-start(bf16[2048,256]{1,0:T(8,128)(2,1)S(1)} %collective-permute-done.2), channel_id=1, source_target_pairs={{0,4},{4,8},{8,12},{12,16},{16,20},{20,24},{24,28},{28,0},{1,5},{5... | collective-permute-start | bytes 3145736 | tf_op jit(solution)/shard_map/ppermute | solution.py:72
  342.7 1.0 copy-start.5
  343.7 49.1 %collective-permute-start.4 = (bf16[2048,256]{1,0:T(8,128)(2,1)S(1)}, bf16[2048,256]{1,0:T(8,128)(2,1)S(1)}, u32[]{:S(2)}, u32[]{:S(2)}) collective-permute-start(bf16[2048,256]{1,0:T(8,128)(2,1)S(1)} %collective-permute-done.3), channel_id=1, source_target_pairs={{0,4},{4,8},{8,12},{12,16},{16,20},{20,24},{24,28},{28,0},{1,5},{5... | collective-permute-start | bytes 3145736 | tf_op jit(solution)/shard_map/ppermute | solution.py:72
  392.7 1.0 copy-start.7
  393.7 27.3 %collective-permute-start.5 = (bf16[2048,256]{1,0:T(8,128)(2,1)S(1)}, bf16[2048,256]{1,0:T(8,128)(2,1)}, u32[]{:S(2)}, u32[]{:S(2)}) collective-permute-start(bf16[2048,256]{1,0:T(8,128)(2,1)S(1)} %collective-permute-done.4), channel_id=1, source_target_pairs={{0,4},{4,8},{8,12},{12,16},{16,20},{20,24},{24,28},{28,0},{1,5},{5... | collective-permute-start | bytes 3145736 | tf_op jit(solution)/shard_map/ppermute | solution.py:72
  421.0 24.7 %collective-permute-start.6 = (bf16[2048,256]{1,0:T(8,128)(2,1)}, bf16[2048,256]{1,0:T(8,128)(2,1)}, u32[]{:S(2)}, u32[]{:S(2)}) collective-permute-start(bf16[2048,256]{1,0:T(8,128)(2,1)} %collective-permute-done.5), channel_id=1, source_target_pairs={{0,4},{4,8},{8,12},{12,16},{16,20},{20,24},{24,28},{28,0},{1,5},{5... | collective-permute-start | bytes 3145736 | tf_op jit(solution)/shard_map/ppermute | solution.py:72
  421.0 34.1 %copy-start.4 = (bf16[2048,256]{1,0:T(8,128)(2,1)S(1)}, bf16[2048,256]{1,0:T(8,128)(2,1)}, u32[]{:S(2)}) copy-start(bf16[2048,256]{1,0:T(8,128)(2,1)} %copy-done.3) | copy-start | bytes 3145732
  421.0 35.2 %copy-start.2 = (bf16[2048,256]{1,0:T(8,128)(2,1)S(1)}, bf16[2048,256]{1,0:T(8,128)(2,1)}, u32[]{:S(2)}) copy-start(bf16[2048,256]{1,0:T(8,128)(2,1)} %copy-done.1) | copy-start | bytes 3145732
  450.4 13.8 %copy-start.8 = (bf16[2048,256]{1,0:T(8,128)(2,1)S(1)}, bf16[2048,256]{1,0:T(8,128)(2,1)}, u32[]{:S(2)}) copy-start(bf16[2048,256]{1,0:T(8,128)(2,1)} %copy-done.7) | copy-start | bytes 3145732
  452.8 12.5 %copy-start.6 = (bf16[2048,256]{1,0:T(8,128)(2,1)S(1)}, bf16[2048,256]{1,0:T(8,128)(2,1)}, u32[]{:S(2)}) copy-start(bf16[2048,256]{1,0:T(8,128)(2,1)} %copy-done.5) | copy-start | bytes 3145732
Sparse Core Ops, SparseCore 0:
  9.5 51.9 all-gather.4
  63.5 47.6 all-gather.6
  175.7 20.1 all-gather.8
  197.9 189.2 all-gather.10
  487.4 28.7 reduce-scatter.1
